TPU v7x, 32 devices: a whole 2x2x4 slice. The times are simulated.
32 devices in a mesh: ep: 8 (over z, x), tp: 4 (over y, core).
Axes of the slice: x: 2, y: 2, z: 4, core: 2. Of those that a mesh axis runs over, the one named last changes fastest.
Arguments:
- residual: bfloat16 [256, 2048], P('ep'), may hold values from -6 to 6
- routes: int32 [256, 4], P('ep'), may hold values from 0 to 7, as said below
- lengths: int32 [256], P('ep'), may hold values from 1 to 512, as said below
- key_cache: bfloat16 [256, 512, 4, 128], P('ep', None, 'tp'), may hold values from -6 to 6
- value_cache: bfloat16 [256, 512, 4, 128], P('ep', None, 'tp'), may hold values from -6 to 6
- mix_gain: float32 [2048], replicated, may hold values from 0.1 to 1.9
- w_query: bfloat16 [2048, 2048], P(None, 'tp'), may hold values from -0.125 to 0.125
- w_out: bfloat16 [2048, 2048], P('tp'), may hold values from -0.375 to 0.375
- head_bias: float32 [16], P('tp'), may hold values from -7 to -1
- moe_gain: float32 [2048], replicated, may hold values from 0.1 to 1.9
- w_group: bfloat16 [2048, 1], replicated, may hold values from -0.02734375 to 0.02734375
- w_expert: bfloat16 [2048, 8], replicated, may hold values from -0.02734375 to 0.02734375
- expert_gate: bfloat16 [8, 2048, 1024], P('ep', None, 'tp'), may hold values from -0.125 to 0.125
- expert_up: bfloat16 [8, 2048, 1024], P('ep', None, 'tp'), may hold values from -0.125 to 0.125
- expert_down: bfloat16 [8, 1024, 2048], P('ep', 'tp'), may hold values from -3 to 3
Outputs:
- layer_out: bfloat16 [256, 2048], P('ep', 'tp')
Inputs may be any that keep to these rules, and one draw needn't show every extreme that they name: `routes`: each row names 4 different experts, all in one group of 8 consecutive experts. Within the rows of one device (aligned blocks of 32 rows) no expert is named more than 16 times, and some expert is named exactly 16 times in every block. `lengths`: some sequence has 512 cached positions in every draw.
All inputs are finite; a program needn't handle non-finite values.
Results may differ from a plain program's by a relative error of at most 0.02.
Values may be sent and summed in bfloat16 or wider, within the bound.
A program may use at most 64 MiB of HBM per device.

v0:
```python
import jax
import jax.numpy as jnp
from jax import lax
from jax.sharding import PartitionSpec as P

GROUP_SIZE = 8
TOPK = 4


EPSILON = 1e-06


def rms_scale(tokens, gains):
    values = tokens.astype(jnp.float32)
    inverse = lax.rsqrt(jnp.mean(values * values, axis=-1, keepdims=True) + EPSILON)
    return (values * inverse * gains).astype(jnp.bfloat16)


def stick_read(queries, key_rows, value_rows, head_bias, lengths):
    seq_count = queries.shape[0]
    key_heads = key_rows.shape[2]
    head_size = key_rows.shape[3]
    per_key = head_bias.shape[0] // key_heads
    grouped = queries.reshape(seq_count, key_heads, per_key, head_size)
    scores = jnp.einsum(
        "tkgd,tlkd->tkgl", grouped, key_rows, preferred_element_type=jnp.float32
    ) * head_size ** (-0.5)
    scores = scores + head_bias.reshape(1, key_heads, per_key, 1)
    inside = lax.broadcasted_iota(jnp.int32, scores.shape, 3) < lengths[:, None, None, None]
    remain = jnp.where(inside, jax.nn.log_sigmoid(-scores), 0.0)
    later_sum = lax.cumsum(remain, axis=3, reverse=True) - remain
    weights = jnp.where(inside, jnp.exp(jax.nn.log_sigmoid(scores) + later_sum), 0.0).astype(
        jnp.bfloat16
    )
    mixture = jnp.einsum("tkgl,tlkd->tkgd", weights, value_rows, preferred_element_type=jnp.float32)
    return mixture.astype(jnp.bfloat16).reshape(seq_count, key_heads * per_key * head_size)


def per_device(
    residual,
    routes,
    lengths,
    key_cache,
    value_cache,
    mix_gain,
    w_query,
    w_out,
    head_bias,
    moe_gain,
    w_group,
    w_expert,
    expert_gate,
    expert_up,
    expert_down,
):
    seq_count = residual.shape[0]
    width = residual.shape[1]
    own_width = width // lax.axis_size("tp")
    own_start = lax.axis_index("tp") * own_width
    normed = rms_scale(residual, mix_gain)
    queries = jnp.dot(normed, w_query, preferred_element_type=jnp.float32).astype(jnp.bfloat16)
    attended = stick_read(queries, key_cache, value_cache, head_bias, lengths)
    head_part = (
        jnp.dot(attended, w_out, preferred_element_type=jnp.float32)
        .astype(jnp.bfloat16)
        .astype(jnp.float32)
    )
    attn_own = lax.psum_scatter(
        head_part.astype(jnp.bfloat16), "tp", scatter_dimension=1, tiled=True
    )
    res_own = lax.dynamic_slice_in_dim(residual, own_start, own_width, 1)
    mid_own = (res_own.astype(jnp.float32) + attn_own.astype(jnp.float32)).astype(jnp.bfloat16)
    mid_values = mid_own.astype(jnp.float32)
    squares = lax.psum(jnp.sum(mid_values * mid_values, axis=1), "tp")
    inverse = lax.rsqrt(squares / width + EPSILON)
    gain_own = lax.dynamic_slice_in_dim(moe_gain, own_start, own_width, 0)
    send_rows = (mid_values * inverse[:, None] * gain_own[None, :]).astype(jnp.bfloat16)
    hidden_in = lax.all_gather(send_rows, "tp", axis=1, tiled=True)
    expert_count = w_expert.shape[1]
    group_count = w_group.shape[1]
    group_prob = jax.nn.softmax(
        jnp.dot(hidden_in, w_group, preferred_element_type=jnp.float32), axis=-1
    )
    expert_logit = jnp.dot(hidden_in, w_expert, preferred_element_type=jnp.float32)
    expert_ids = jnp.arange(expert_count, dtype=jnp.int32)
    chosen = routes[:, :, None] == expert_ids[None, None, :]
    picked = jnp.sum(jnp.where(chosen, expert_logit[:, None, :], 0.0), axis=2)
    group_hot = routes[:, :1] // GROUP_SIZE == jnp.arange(group_count, dtype=jnp.int32)[None, :]
    top_prob = jnp.sum(jnp.where(group_hot, group_prob, 0.0), axis=1, keepdims=True)
    share = jax.nn.softmax(picked, axis=1) * top_prob
    group_most = min(seq_count, max(4, 2 * seq_count // group_count))
    capacity = group_most * TOPK // GROUP_SIZE
    flat_hot = chosen.reshape(seq_count * TOPK, expert_count).astype(jnp.int32)
    earlier = jnp.cumsum(flat_hot, axis=0, dtype=jnp.int32) - flat_hot
    slot = jnp.sum(earlier * flat_hot, axis=1, dtype=jnp.int32)
    target = routes.reshape(-1) * capacity + slot
    placing = target[:, None] == jnp.arange(expert_count * capacity, dtype=jnp.int32)[None, :]
    placing = placing.reshape(seq_count, TOPK, expert_count * capacity)
    token_place = jnp.sum(placing.astype(jnp.int32), axis=1).astype(jnp.bfloat16)
    outgoing = jnp.einsum("sq,sd->qd", token_place, send_rows, preferred_element_type=jnp.float32)
    outgoing = outgoing.astype(jnp.bfloat16).reshape(expert_count, capacity, send_rows.shape[1])
    local_experts = expert_gate.shape[0]
    arrived = lax.all_to_all(outgoing, "ep", split_axis=0, concat_axis=0, tiled=True)
    arrived = lax.all_gather(arrived, "tp", axis=2, tiled=True)
    sources = arrived.shape[0] // local_experts
    batch_rows = arrived.reshape(sources, local_experts, arrived.shape[1], arrived.shape[2])
    gate = jnp.einsum("nxcd,xdf->nxcf", batch_rows, expert_gate, preferred_element_type=jnp.float32)
    upward = jnp.einsum("nxcd,xdf->nxcf", batch_rows, expert_up, preferred_element_type=jnp.float32)
    active = (jax.nn.silu(gate) * upward).astype(jnp.bfloat16)
    partial_value = jnp.einsum(
        "nxcf,xfd->nxcd", active, expert_down, preferred_element_type=jnp.float32
    )
    partial_value = partial_value.astype(jnp.bfloat16).astype(jnp.float32)
    partial_value = partial_value.reshape(
        arrived.shape[0], arrived.shape[1], partial_value.shape[3]
    )
    summed = lax.psum_scatter(
        partial_value.astype(jnp.bfloat16), "tp", scatter_dimension=2, tiled=True
    )
    returned = lax.all_to_all(summed, "ep", split_axis=0, concat_axis=0, tiled=True)
    combine = jnp.einsum(
        "sk,skq->sq", share, placing.astype(jnp.float32), precision=lax.Precision.HIGHEST
    )
    moe = jnp.dot(
        combine,
        returned.reshape(expert_count * capacity, own_width).astype(jnp.float32),
        precision=lax.Precision.HIGHEST,
    )
    return (mid_own.astype(jnp.float32) + moe).astype(jnp.bfloat16)


def solution(mesh):
    in_specs = (
        P("ep", None),
        P("ep", None),
        P("ep"),
        P("ep", None, "tp", None),
        P("ep", None, "tp", None),
        P(),
        P(None, "tp"),
        P("tp", None),
        P("tp"),
        P(),
        P(),
        P(),
        P("ep", None, "tp"),
        P("ep", None, "tp"),
        P("ep", "tp", None),
    )
    out_specs = P("ep", "tp")
    return jax.shard_map(
        per_device, mesh=mesh, in_specs=in_specs, out_specs=out_specs, check_vma=False
    )
```

profile of v0, /device:TPU:0, one launch (start us, length us, event | category | flops | bytes accessed | tf_op | source)
XLA Modules:
  0.0 132.4 jit_solution(12256758625774551817)
XLA Ops:
  6.5 1.2 fusion.28
  7.7 2.2 %convolution_convert_fusion.3 = bf16[32,512]{1,0:T(8,128)(2,1)S(1)} fusion(bf16[2048,512]{1,0:T(8,128)(2,1)} %param.21, bf16[32,2048]{1,0:T(8,128)(2,1)} %param.15, f32[2048]{0:T(1024)} %param.20, f32[32]{0:T(128)S(1)} %add_rsqrt_fusion.1), kind=kOutput, calls=%fused_computation.16 | convolution fusion | flops 67387392 | bytes 2269312 | tf_op jit(solution)/shard_map/dot_general | solution.py:61
  10.0 0.0 copy-start.3
  10.0 3.4 %fusion.37 = (f32[32,4,512]{2,1,0:T(4,128)S(1)}, f32[32,4,512]{2,1,0:T(4,128)S(1)}) fusion(s32[32]{0:T(128)} %param.17, f32[4]{0:T(128)} %param.23, bf16[32,4,128]{2,1,0:T(4,128)(2,1)S(1)} %reshape.157, bf16[32,512,1,128]{3,1,2,0:T(8,128)(2,1)} %param.18), kind=kOutput, calls=%fused_computation.41 | convolution fusion | flops 17498112 | bytes 4751504 | tf_op jit(solution)/shard_map/tkgd,tlkd->tkgl/dot_general | solution.py:25
  13.4 0.2 reshape.159
  13.6 0.1 copy.41
  13.7 19.9 %reduce-window.6 = f32[32,1,4,4,128]{4,0,2,1,3:T(8,128)S(1)} reduce-window(f32[32,1,4,4,128]{4,0,2,1,3:T(8,128)S(1)} %copy.41, f32[]{:T(128)} %constant.45.clone.1), window={size=1x1x1x1x128 pad=0_0x0_0x0_0x0_0x0_127}, to_apply=%region_1.2 | reduce-window | flops 8323072 | bytes 524292 | tf_op jit(solution)/shard_map/reduce-window
  33.6 0.2 copy.42
  33.8 0.2 copy.43
  34.0 0.1 copy.44
  34.1 0.2 broadcast.61
  34.3 0.2 reshape.163
  34.5 0.2 reshape.160
  34.6 0.0 copy-start.2
  34.7 3.2 %fusion.14 = bf16[32,4,128]{2,1,0:T(4,128)(2,1)S(1)} fusion(bf16[32,512,1,128]{3,1,2,0:T(8,128)(2,1)} %param.19, f32[32,4,512]{2,1,0:T(4,128)S(1)} %reshape.160, f32[32,4,512]{2,1,0:T(4,128)S(1)} %reshape.163, f32[32,4,512]{2,1,0:T(4,128)S(1)} %get-tuple-element.8, s32[32]{0:T(128)S(1)} %copy-done.3), kind=kOutput, calls=%fused_computation.17 | convolution fusion | flops 18235392 | bytes 5013632 | tf_op jit(solution)/shard_map/tkgl,tlkd->tkgd/dot_general | solution.py:35
  37.9 1.1 convolution_convert_fusion.1
  39.0 0.0 reduce-scatter.3.cloned.1.call-update
  39.0 0.0 reduce-scatter.5.cloned.1.call-start
  39.1 0.0 copy-done.2
  39.1 0.1 copy.45
  39.2 0.1 eq.44
  39.3 0.1 fusion.53
  39.4 0.2 reduce_window_sum.25
  39.6 0.2 select_reduce_fusion
  39.7 0.1 reduce_sum.69
  39.8 0.1 copy.46
  39.9 0.8 dynamic_slice.7
  40.7 0.1 convert_reduce_fusion
  40.8 20.8 %reduce-scatter.3.cloned.1.call-done = bf16[32,512]{1,0:T(8,128)(2,1)} async-done(((bf16[32,2048]{1,0:T(8,128)(2,1)}), bf16[32,512]{1,0:T(8,128)(2,1)}) %reduce-scatter.3.cloned.1.call-update) | async-done | bytes 32784 | tf_op jit(solution)/shard_map/reduce_scatter | solution.py:68
  61.6 0.9 fusion.49
  62.5 5.8 %psum.7 = f32[32]{0:T(128)S(1)} all-reduce(f32[32]{0:T(128)S(1)} %get-tuple-element.5), channel_id=1, replica_groups=mesh['ep'=8,'tp'=4] {'tp'}, use_global_device_ids=true, to_apply=%region_5.6 | all-reduce | flops 32 | bytes 256 | tf_op jit(solution)/shard_map/psum | solution.py:74
  68.3 0.1 fusion.51
  68.3 0.2 convolution_convert_fusion.2
  68.6 12.8 %all_to_all.10 = bf16[8,16,512]{2,1,0:T(8,128)(2,1)S(1)} all-to-all(bf16[8,16,512]{2,1,0:T(8,128)(2,1)S(1)} %bitcast.105), channel_id=1, replica_groups=mesh['ep'=8,'tp'=4] {'ep'}, dimensions={0} | all-to-all | bytes 262144 | tf_op jit(solution)/shard_map/all_to_all | solution.py:103
  81.4 6.5 %all_gather.7 = bf16[8,16,2048]{2,1,0:T(8,128)(2,1)S(1)} all-gather(bf16[8,16,512]{2,1,0:T(8,128)(2,1)S(1)} %all_to_all.10), channel_id=1, replica_groups=mesh['ep'=8,'tp'=4] {'tp'}, dimensions={2}, use_global_device_ids=true | all-gather | bytes 655360 | tf_op jit(solution)/shard_map/all_gather | solution.py:104
  87.9 1.5 %convolution_bitcast_fusion.1 = f32[8,1,16,256]{3,2,0,1:T(8,128)S(1)} fusion(bf16[8,16,2048]{2,1,0:T(8,128)(2,1)S(1)} %all_gather.7, bf16[1,2048,256]{2,1,0:T(8,128)(2,1)} %param.27), kind=kOutput, calls=%fused_computation.11 | convolution fusion | flops 134217728 | bytes 1703936 | tf_op jit(solution)/shard_map/nxcd,xdf->nxcf/dot_general | solution.py:107
  89.4 3.1 %convolution_convert_fusion = bf16[8,16,2048]{2,1,0:T(8,128)(2,1)} fusion(bf16[1,256,2048]{2,1,0:T(8,128)(2,1)} %param.29, bf16[8,16,2048]{2,1,0:T(8,128)(2,1)S(1)} %all_gather.7, bf16[1,2048,256]{2,1,0:T(8,128)(2,1)} %param.28, f32[8,1,16,256]{3,2,0,1:T(8,128)S(1)} %convolution_bitcast_fusion.1), kind=kOutput, calls=%fused_computation.4 | convolution fusion | flops 268894208 | bytes 3276800 | tf_op jit(solution)/shard_map/nxcf,xfd->nxcd/dot_general | solution.py:110
  92.5 0.0 reduce-scatter.5.cloned.1.call-update
  92.5 0.1 iota_compare_fusion.1
  92.6 5.4 %all_gather.6 = bf16[32,2048]{1,0:T(8,128)(2,1)S(1)} all-gather(bf16[32,512]{1,0:T(8,128)(2,1)S(1)} %fusion.51), channel_id=1, replica_groups=mesh['ep'=8,'tp'=4] {'tp'}, dimensions={1}, use_global_device_ids=true | all-gather | bytes 163840 | tf_op jit(solution)/shard_map/all_gather | solution.py:78
  98.1 0.1 fusion.63
  98.3 0.2 fusion.22
  98.4 13.4 %reduce-scatter.5.cloned.1.call-done = bf16[8,16,512]{2,1,0:T(8,128)(2,1)} async-done(((bf16[8,16,2048]{2,1,0:T(8,128)(2,1)}), bf16[8,16,512]{2,1,0:T(8,128)(2,1)}) %reduce-scatter.5.cloned.1.call-update) | async-done | bytes 131088 | tf_op jit(solution)/shard_map/reduce_scatter | solution.py:117
  111.9 5.5 %all-to-all-start.1 = ((bf16[8,16,512]{2,1,0:T(8,128)(2,1)}), bf16[8,16,512]{2,1,0:T(8,128)(2,1)S(1)}, u32[]{:S(2)}, u32[]{:S(2)}) async-start(bf16[8,16,512]{2,1,0:T(8,128)(2,1)} %reduce-scatter.5.cloned.1.call-done), calls=%async_computation.3 | async-start | bytes 262144 | tf_op jit(solution)/shard_map/all_to_all | solution.py:120
  117.4 0.1 copy.47
  117.5 0.2 fusion.54
  117.7 7.0 %all-to-all-done.1 = bf16[8,16,512]{2,1,0:T(8,128)(2,1)S(1)} async-done(((bf16[8,16,512]{2,1,0:T(8,128)(2,1)}), bf16[8,16,512]{2,1,0:T(8,128)(2,1)S(1)}, u32[]{:S(2)}, u32[]{:S(2)}) %all-to-all-start.1) | async-done | bytes 131104 | tf_op jit(solution)/shard_map/all_to_all | solution.py:120
  124.7 0.8 fusion.13
  (18 shorter events, 0.2 us)
Async XLA Ops:
  6.5 31.3 %copy-start = (bf16[512,2048]{1,0:T(8,128)(2,1)S(1)}, bf16[512,2048]{1,0:T(8,128)(2,1)}, u32[]{:S(2)}) copy-start(bf16[512,2048]{1,0:T(8,128)(2,1)} %param.22) | copy-start | bytes 6291460
  6.5 55.1 %reduce-scatter.3.cloned.1.call-start = ((), (), s32[]{:S(2)}) async-start(), calls=%async_computation.4 | async-start | bytes 163840 | tf_op jit(solution)/shard_map/reduce_scatter | solution.py:68
  10.0 24.7 %copy-start.3 = (s32[32]{0:T(128)S(1)}, s32[32]{0:T(128)}, u32[]{:S(2)}) copy-start(s32[32]{0:T(128)} %param.17) | copy-start | bytes 388
  34.6 4.5 %copy-start.2 = (s32[32,4]{0,1:T(4,128)S(1)}, s32[32,4]{0,1:T(4,128)}, u32[]{:S(2)}) copy-start(s32[32,4]{0,1:T(4,128)} %param.16) | copy-start | bytes 1540
  39.0 59.1 %copy-start.1 = (bf16[2048,8]{0,1:T(8,128)(2,1)S(1)}, bf16[2048,8]{0,1:T(8,128)(2,1)}, u32[]{:S(2)}) copy-start(bf16[2048,8]{0,1:T(8,128)(2,1)} %param.26) | copy-start | bytes 98308
  39.0 59.3 %copy-start.4 = (bf16[2048,1]{0,1:T(2,128)(2,1)S(1)}, bf16[2048,1]{0,1:T(2,128)(2,1)}, u32[]{:S(2)}) copy-start(bf16[2048,1]{0,1:T(2,128)(2,1)} %param.25) | copy-start | bytes 12292
  39.0 72.8 %reduce-scatter.5.cloned.1.call-start = ((), (), s32[]{:S(2)}) async-start(), calls=%async_computation.5 | async-start | bytes 655360 | tf_op jit(solution)/shard_map/reduce_scatter | solution.py:117
  111.9 12.8 %all-to-all-start.1 = ((bf16[8,16,512]{2,1,0:T(8,128)(2,1)}), bf16[8,16,512]{2,1,0:T(8,128)(2,1)S(1)}, u32[]{:S(2)}, u32[]{:S(2)}) async-start(bf16[8,16,512]{2,1,0:T(8,128)(2,1)} %reduce-scatter.5.cloned.1.call-done), calls=%async_computation.3 | async-start | bytes 262144 | tf_op jit(solution)/shard_map/all_to_all | solution.py:120
Sparse Core Ops, SparseCore 0:
  39.1 22.4 reduce-scatter.2
  92.7 19.1 reduce-scatter.4
where the time goes:
time: 133 us; the launch traced here: 132 us
  waiting for transfers between devices  41.3 us (31%)
  blocking collectives  30.5 us (23%)
  other arithmetic  22.8 us (17%)
  matrix products  16.2 us (12%)
  between operations  13.6 us (10%)
  starting transfers between devices  5.54 us (4%)
  local copies, waits for them, and re-layouts  2.47 us (2%)
    reduce_scatter x1, waiting for transfers between devices, per_device(): lax.psum_scatter(head_part.astype(jnp.bfloat16), 'tp', scatter_dimension=...  20.8 us
    another operation x2, other arithmetic  20 us
    reduce_scatter x1, waiting for transfers between devices, per_device(): lax.psum_scatter(partial_value.astype(jnp.bfloat16), 'tp', scatter_dimens...  13.4 us
    all_to_all x1, blocking collectives, per_device(): lax.all_to_all(outgoing, 'ep', split_axis=0, concat_axis=0, tiled=True)  12.8 us
    all_to_all x1, waiting for transfers between devices, per_device(): lax.all_to_all(summed, 'ep', split_axis=0, concat_axis=0, tiled=True)  6.99 us
    all_gather x1, blocking collectives, per_device(): arrived = lax.all_gather(arrived, 'tp', axis=2, tiled=True)  6.49 us
    psum x1, blocking collectives, per_device(): squares = lax.psum(jnp.sum(mid_values * mid_values, axis=1), 'tp')  5.76 us
    all_to_all x1, starting transfers between devices, per_device(): lax.all_to_all(summed, 'ep', split_axis=0, concat_axis=0, tiled=True)  5.5 us
  transfers between devices with their start and end apart: 3, of which 3 were waited for; matrix products, arithmetic and copies ran while one was open for 2% of the time, Pallas kernels for 0%

commit v1 on v0

v1 whole, which is shorter than its diff:
```python
import functools

import jax
import jax.numpy as jnp
from jax import lax
from jax.experimental import pallas as pl
from jax.experimental.pallas import tpu as pltpu
from jax.sharding import PartitionSpec as P

GROUP_SIZE = 8
TOPK = 4
EPSILON = 1e-06
MESH = pl.DeviceIdType.MESH
BF = jnp.bfloat16
F32 = jnp.float32
KEY_CHUNKS = 4
NT = (((1,), (1,)), ((), ()))
TN = (((0,), (0,)), ((), ()))


def split3(values):
    first = values.astype(BF)
    rest = values - first.astype(F32)
    second = rest.astype(BF)
    third = (rest - second.astype(F32)).astype(BF)
    return first, second, third


def remote(src, dst, send, recv, device):
    return pltpu.make_async_remote_copy(
        src_ref=src, dst_ref=dst, send_sem=send, recv_sem=recv,
        device_id=device, device_id_type=MESH,
    )


def kernel(
    n_ep, n_tp, capacity,
    lens_ref, bias_ref, routes_ref, wexp_ref, wgrp_ref,
    mixg_hbm, moeg_hbm, res_hbm, wq_hbm, key_hbm, value_hbm, wo_hbm, wg_hbm, wu_hbm, wd_hbm,
    out_ref,
    mixg, moeg, res, wq, keys, values, wo, wg, wu, wd,
    qs, scores, sticks, att, head_send, head_recv, mid_all, slots, full,
    part_send, part_recv, pair_send, pair_recv, ret_send, ret_recv,
    small_sem, weight_sem, key_sem, value_sem,
    head_ss, head_rs, mid_ss, mid_rs, disp_ss, disp_rs,
    core_ss, core_rs, cross_ss, cross_rs, fwd_ss, fwd_rs,
    part_ss, part_rs, pair_ss, pair_rs, ret_ss, ret_rs,
):
    ep = lax.axis_index("ep")
    tp = lax.axis_index("tp")
    near = tp + 1 - 2 * (tp % 2)
    far = (tp + 2) % n_tp
    diag = (near + 2) % n_tp
    seqs, width = res.shape
    own = width // n_tp
    heads = bias_ref.shape[0] // seqs
    size = keys.shape[2]
    experts = wexp_ref.shape[0]

    def ep_peer(d):
        return lax.rem(ep + d, n_ep)

    def ep_source(d):
        return lax.rem(ep + n_ep - d, n_ep)

    loads = [
        pltpu.make_async_copy(src, dst, small_sem.at[i])
        for i, (src, dst) in enumerate(((res_hbm, res), (mixg_hbm, mixg), (moeg_hbm, moeg)))
    ]
    weights = [
        pltpu.make_async_copy(src, dst, weight_sem.at[i])
        for i, (src, dst) in enumerate(
            ((wq_hbm, wq), (wo_hbm, wo), (wg_hbm, wg), (wu_hbm, wu), (wd_hbm, wd))
        )
    ]
    step = seqs // KEY_CHUNKS
    key_loads = []
    value_loads = []
    for c in range(KEY_CHUNKS):
        rows = pl.ds(c * step, step)
        key_loads.append(pltpu.make_async_copy(key_hbm.at[rows], keys.at[rows], key_sem.at[c]))
        value_loads.append(
            pltpu.make_async_copy(value_hbm.at[rows], values.at[rows], value_sem.at[c])
        )
    for copy in loads + weights[:1] + key_loads + value_loads + weights[1:]:
        copy.start()

    barrier = pltpu.get_barrier_semaphore()
    for d in range(1, n_tp):
        pl.semaphore_signal(
            barrier, inc=1, device_id={"tp": lax.rem(tp + d, n_tp)}, device_id_type=MESH
        )

    @pl.loop(1, n_ep)
    def _(d):
        pl.semaphore_signal(barrier, inc=1, device_id={"ep": ep_peer(d)}, device_id_type=MESH)

    for copy in loads:
        copy.wait()
    tokens = res[...].astype(F32)
    inverse = lax.rsqrt(jnp.sum(tokens * tokens, axis=1, keepdims=True) / width + EPSILON)
    normed = (tokens * inverse * mixg[...]).astype(BF)
    weights[0].wait()
    queries = jnp.dot(normed, wq[...], preferred_element_type=F32).astype(BF).astype(F32)
    for h in range(heads):
        qs[pl.ds(h, seqs, stride=heads), :] = queries[:, h * size:(h + 1) * size]
    per = 8 // heads
    row_of = lax.broadcasted_iota(jnp.int32, (8, 1), 0)
    for t in range(0, seqs, per):
        if t % step == 0:
            key_loads[t // step].wait()
        rows = qs[t * heads:t * heads + 8, :].astype(BF)
        total = None
        for j in range(per):
            term = lax.dot_general(rows, keys[t + j], NT, preferred_element_type=F32)
            total = term if total is None else jnp.where(row_of < j * heads, total, term)
        scores[t * heads:t * heads + 8, :] = total
    length = keys.shape[1]
    z = scores[...] * size ** (-0.5) + bias_ref[...]
    inside = lax.broadcasted_iota(jnp.int32, z.shape, 1) < lens_ref[...]
    low = jnp.log1p(jnp.exp(-jnp.abs(z)))
    remain = jnp.where(inside, -(jnp.maximum(z, 0.0) + low), 0.0)
    after = (
        lax.broadcasted_iota(jnp.int32, (length, length), 0)
        > lax.broadcasted_iota(jnp.int32, (length, length), 1)
    ).astype(F32).astype(BF)
    later = None
    for term in split3(remain):
        value = jnp.dot(term, after, preferred_element_type=F32)
        later = value if later is None else later + value
    sticks[...] = jnp.where(inside, jnp.exp(jnp.minimum(z, 0.0) - low + later), 0.0)
    for t in range(0, seqs, per):
        if t % step == 0:
            value_loads[t // step].wait()
        rows = sticks[t * heads:t * heads + 8, :].astype(BF)
        total = None
        for j in range(per):
            term = jnp.dot(rows, values[t + j], preferred_element_type=F32)
            total = term if total is None else jnp.where(row_of < j * heads, total, term)
        att[t * heads:t * heads + 8, :] = total
    attended = jnp.concatenate(
        [att[pl.ds(h, seqs, stride=heads), :].astype(BF) for h in range(heads)], axis=1
    )
    weights[1].wait()
    for p in range(n_tp):
        head_send[p] = jnp.dot(
            attended, wo[:, p * own:(p + 1) * own], preferred_element_type=F32
        ).astype(BF)

    pl.semaphore_wait(barrier, n_tp - 1 + n_ep - 1)
    head_copies = []
    for d in range(1, n_tp):
        peer = lax.rem(tp + d, n_tp)
        head_copies.append(
            remote(head_send.at[peer], head_recv.at[d], head_ss.at[d], head_rs.at[d], {"tp": peer})
        )
        head_copies[-1].start()

    routes = routes_ref[...]
    expert_row = lax.broadcasted_iota(jnp.int32, (experts, seqs), 0)
    chosen = jnp.zeros((experts, seqs), F32)
    for k in range(TOPK):
        chosen = chosen + jnp.where(routes[k:k + 1, :] == expert_row, 1.0, 0.0)
    before = (
        lax.broadcasted_iota(jnp.int32, (seqs, seqs), 0)
        < lax.broadcasted_iota(jnp.int32, (seqs, seqs), 1)
    ).astype(F32).astype(BF)
    earlier = jnp.dot(chosen.astype(BF), before, preferred_element_type=F32)
    slot_of = jnp.where(chosen > 0.5, earlier, -1.0)
    slot_row = lax.broadcasted_iota(jnp.int32, (experts, capacity, seqs), 1).astype(F32)
    place = jnp.where(
        jnp.broadcast_to(slot_of[:, None, :], slot_row.shape) == slot_row, 1.0, 0.0
    ).reshape(experts * capacity, seqs)

    attn = head_send[tp].astype(F32)
    for copy in head_copies:
        copy.wait_recv()
    for d in range(1, n_tp):
        attn = attn + head_recv[d].astype(F32)
    own_columns = pl.ds(pl.multiple_of(tp * own, own), own)
    mid_own = (
        res[:, own_columns].astype(F32) + attn.astype(BF).astype(F32)
    ).astype(BF)
    routed = jnp.dot(place.astype(BF), mid_own, preferred_element_type=F32).astype(BF)
    slots[...] = routed.reshape(experts, capacity, own)
    mid_all[tp] = mid_own

    def dispatch(d):
        return remote(
            slots.at[ep_peer(d)], full.at[tp, ep], disp_ss.at[d], disp_rs.at[d],
            {"ep": ep_peer(d)},
        )

    @pl.loop(1, n_ep)
    def _(d):
        dispatch(d).start()

    full[tp, ep] = slots[ep]
    mid_copies = []
    for d in range(1, n_tp):
        peer = lax.rem(tp + d, n_tp)
        mid_copies.append(
            remote(mid_all.at[tp], mid_all.at[tp], mid_ss.at[d], mid_rs.at[d], {"tp": peer})
        )

    def to_core(d):
        at = (tp, ep_source(d))
        return remote(full.at[at], full.at[at], core_ss.at[d], core_rs.at[d], {"tp": near})

    def to_far(d):
        at = (tp, ep_source(d))
        return remote(full.at[at], full.at[at], cross_ss.at[d], cross_rs.at[d], {"tp": far})

    def onward(d):
        at = (far, ep_source(d))
        return remote(full.at[at], full.at[at], fwd_ss.at[d], fwd_rs.at[d], {"tp": near})

    to_far(0).start()
    to_core(0).start()

    @pl.loop(1, n_ep)
    def _(d):
        dispatch(d).wait_recv()
        to_far(d).start()
        to_core(d).start()

    for copy in mid_copies:
        copy.start()

    @pl.loop(0, n_ep)
    def _(d):
        to_far(d).wait_recv()
        onward(d).start()

    for copy in weights[2:]:
        copy.wait()

    @pl.loop(0, n_ep)
    def _(d):
        to_core(d).wait_recv()

    @pl.loop(0, n_ep)
    def _(d):
        onward(d).wait_recv()

    rows = n_ep * capacity
    squares = jnp.zeros((rows, 1), F32)
    for p in range(n_tp):
        block = full[p].reshape(rows, own).astype(F32)
        squares = squares + jnp.sum(block * block, axis=1, keepdims=True)
    inverse = lax.rsqrt(squares / width + EPSILON)
    gate = None
    for p in range(n_tp):
        columns = slice(p * own, (p + 1) * own)
        block = full[p].reshape(rows, own).astype(F32)
        hidden = (block * inverse * moeg[:, columns]).astype(BF)
        gate_term = jnp.dot(hidden, wg[columns, :], preferred_element_type=F32)
        up_term = jnp.dot(hidden, wu[columns, :], preferred_element_type=F32)
        gate = gate_term if gate is None else gate + gate_term
        upward = up_term if p == 0 else upward + up_term
    active = (gate / (1.0 + jnp.exp(-gate)) * upward).astype(BF)

    def partial_of(p):
        columns = pl.ds(pl.multiple_of(p * own, own), own)
        value = jnp.dot(active, wd[:, columns], preferred_element_type=F32)
        return value.astype(BF).reshape(n_ep, capacity, own)

    part_copies = []
    for i, peer in enumerate((diag, near)):
        part_send[i] = partial_of(peer)
        part_copies.append(
            remote(part_send.at[i], part_recv.at[i], part_ss.at[i], part_rs.at[i], {"tp": near})
        )
        part_copies[-1].start()
    far_part = partial_of(far).astype(F32)
    part_copies[0].wait_recv()
    pair_send[...] = (far_part + part_recv[0].astype(F32)).astype(BF)

    def pair(d):
        at = ep_source(d)
        return remote(
            pair_send.at[at], pair_recv.at[at], pair_ss.at[d], pair_rs.at[d], {"tp": far}
        )

    @pl.loop(1, n_ep)
    def _(d):
        pair(d).start()

    pair(0).start()
    own_part = partial_of(tp).astype(F32)
    part_copies[1].wait_recv()
    ret_send[...] = own_part + part_recv[1].astype(F32)

    def giving(d):
        at = ep_source(d)
        return remote(slots.at[at], ret_recv.at[ep], ret_ss.at[d], ret_rs.at[d], {"ep": at})

    @pl.loop(1, n_ep)
    def _(d):
        dispatch(d).wait_send()

    @pl.loop(1, n_ep)
    def _(d):
        at = ep_source(d)
        pair(d).wait_recv()
        slots[at] = (ret_send[at] + pair_recv[at].astype(F32)).astype(BF)
        giving(d).start()

    pair(0).wait_recv()
    ret_recv[ep] = (ret_send[ep] + pair_recv[ep].astype(F32)).astype(BF)

    for copy in mid_copies:
        copy.wait_recv()
    squares = jnp.zeros((seqs, 1), F32)
    for p in range(n_tp):
        block = mid_all[p].astype(F32)
        squares = squares + jnp.sum(block * block, axis=1, keepdims=True)
    inverse = lax.rsqrt(squares / width + EPSILON)
    logit = jnp.zeros((experts, seqs), F32)
    group_logit = jnp.zeros((wgrp_ref.shape[0], seqs), F32)
    for p in range(n_tp):
        columns = slice(p * own, (p + 1) * own)
        hidden = (mid_all[p].astype(F32) * inverse * moeg[:, columns]).astype(BF)
        logit = logit + lax.dot_general(
            wexp_ref[:, columns], hidden, NT, preferred_element_type=F32
        )
        group_logit = group_logit + lax.dot_general(
            wgrp_ref[:, columns], hidden, NT, preferred_element_type=F32
        )
    group_exp = jnp.exp(group_logit - jnp.max(group_logit, axis=0, keepdims=True))
    group_prob = group_exp / jnp.sum(group_exp, axis=0, keepdims=True)
    group_row = lax.broadcasted_iota(jnp.int32, group_prob.shape, 0)
    group_of = jnp.zeros((1, seqs), jnp.int32) + lax.shift_right_logical(
        routes[0:1, :], jnp.full((1, seqs), GROUP_SIZE.bit_length() - 1, jnp.int32)
    )
    top_prob = jnp.sum(jnp.where(group_of == group_row, group_prob, 0.0), axis=0, keepdims=True)
    peak = jnp.max(jnp.where(chosen > 0.5, logit, -jnp.inf), axis=0, keepdims=True)
    raised = jnp.where(chosen > 0.5, jnp.exp(jnp.minimum(logit - peak, 0.0)), 0.0)
    share = raised / jnp.sum(raised, axis=0, keepdims=True) * top_prob
    combine = place * jnp.broadcast_to(share[:, None, :], slot_row.shape).reshape(place.shape)

    @pl.loop(1, n_ep)
    def _(d):
        remote(
            slots.at[ep], ret_recv.at[ep_peer(d)], ret_ss.at[d], ret_rs.at[d], {"ep": ep_source(d)}
        ).wait_recv()

    returned = ret_recv[...].reshape(experts * capacity, own)
    moe = None
    for term in split3(combine):
        value = lax.dot_general(term, returned, TN, preferred_element_type=F32)
        moe = value if moe is None else moe + value
    out_ref[...] = (mid_all[tp].astype(F32) + moe).astype(BF)

    for copy in head_copies + mid_copies + part_copies:
        copy.wait_send()

    @pl.loop(0, n_ep)
    def _(d):
        to_core(d).wait_send()
        to_far(d).wait_send()
        onward(d).wait_send()
        pair(d).wait_send()

    @pl.loop(1, n_ep)
    def _(d):
        giving(d).wait_send()


def per_device(
    n_ep, n_tp,
    residual, routes, lengths, key_cache, value_cache, mix_gain, w_query, w_out, head_bias,
    moe_gain, w_group, w_expert, expert_gate, expert_up, expert_down,
):
    seqs, width = residual.shape
    length, size = key_cache.shape[1], key_cache.shape[3]
    heads = head_bias.shape[0]
    experts, groups = w_expert.shape[1], w_group.shape[1]
    assert key_cache.shape[2] == 1 and expert_gate.shape[0] == 1 and n_tp == 4
    assert experts == n_ep
    own = width // n_tp
    units = expert_gate.shape[2]
    most = min(seqs, max(4, 2 * seqs // groups)) * TOPK // GROUP_SIZE
    capacity = -(-most // 16) * 16
    rows = seqs * heads
    vmem = pl.BlockSpec(memory_space=pltpu.VMEM)
    hbm = pl.BlockSpec(memory_space=pltpu.HBM)
    dma = pltpu.SemaphoreType.DMA
    return pl.pallas_call(
        functools.partial(kernel, n_ep, n_tp, capacity),
        out_shape=jax.ShapeDtypeStruct((seqs, own), BF),
        in_specs=[vmem] * 5 + [hbm] * 10,
        out_specs=vmem,
        scratch_shapes=[
            pltpu.VMEM((1, width), F32),
            pltpu.VMEM((1, width), F32),
            pltpu.VMEM((seqs, width), BF),
            pltpu.VMEM(w_query.shape, BF),
            pltpu.VMEM((seqs, length, size), BF),
            pltpu.VMEM((seqs, length, size), BF),
            pltpu.VMEM(w_out.shape, BF),
            pltpu.VMEM((width, units), BF),
            pltpu.VMEM((width, units), BF),
            pltpu.VMEM((units, width), BF),
            pltpu.VMEM((rows, size), F32),
            pltpu.VMEM((rows, length), F32),
            pltpu.VMEM((rows, length), F32),
            pltpu.VMEM((rows, size), F32),
            pltpu.VMEM((n_tp, seqs, own), BF),
            pltpu.VMEM((n_tp, seqs, own), BF),
            pltpu.VMEM((n_tp, seqs, own), BF),
            pltpu.VMEM((n_ep, capacity, own), BF),
            pltpu.VMEM((n_tp, n_ep, capacity, own), BF),
            pltpu.VMEM((2, n_ep, capacity, own), BF),
            pltpu.VMEM((2, n_ep, capacity, own), BF),
            pltpu.VMEM((n_ep, capacity, own), BF),
            pltpu.VMEM((n_ep, capacity, own), BF),
            pltpu.VMEM((n_ep, capacity, own), F32),
            pltpu.VMEM((n_ep, capacity, own), BF),
            dma((3,)), dma((5,)), dma((KEY_CHUNKS,)), dma((KEY_CHUNKS,)),
            dma((n_tp,)), dma((n_tp,)), dma((n_tp,)), dma((n_tp,)),
            dma((n_ep,)), dma((n_ep,)),
            dma((n_ep,)), dma((n_ep,)), dma((n_ep,)), dma((n_ep,)), dma((n_ep,)), dma((n_ep,)),
            dma((2,)), dma((2,)), dma((n_ep,)), dma((n_ep,)), dma((n_ep,)), dma((n_ep,)),
        ],
        compiler_params=pltpu.CompilerParams(
            collective_id=0, has_side_effects=True, vmem_limit_bytes=60 * 1024 * 1024
        ),
        name="decode_step",
    )(
        jnp.repeat(lengths, heads)[:, None],
        jnp.tile(head_bias, seqs)[:, None],
        routes.T,
        w_expert.T,
        w_group.T,
        mix_gain.reshape(1, width),
        moe_gain.reshape(1, width),
        residual,
        w_query,
        key_cache.reshape(seqs, length, size),
        value_cache.reshape(seqs, length, size),
        w_out,
        expert_gate.reshape(width, units),
        expert_up.reshape(width, units),
        expert_down.reshape(units, width),
    )


def solution(mesh):
    in_specs = (
        P("ep", None),
        P("ep", None),
        P("ep"),
        P("ep", None, "tp", None),
        P("ep", None, "tp", None),
        P(),
        P(None, "tp"),
        P("tp", None),
        P("tp"),
        P(),
        P(),
        P(),
        P("ep", None, "tp"),
        P("ep", None, "tp"),
        P("ep", "tp", None),
    )
    return jax.shard_map(
        functools.partial(per_device, mesh.shape["ep"], mesh.shape["tp"]),
        mesh=mesh, in_specs=in_specs, out_specs=P("ep", "tp"), check_vma=False,
    )
```

time: 133 us -> 41.9 us (0.32)
  waiting for transfers between devices: 41.3 us -> 0 us
  Pallas kernels: 0 us -> 37.5 us
  blocking collectives: 30.5 us -> 0 us
  other arithmetic: 22.8 us -> 0 us
  matrix products: 16.2 us -> 0 us
  between operations: 13.6 us -> 0.01 us
  starting transfers between devices: 5.54 us -> 0 us
  local copies, waits for them, and re-layouts: 2.47 us -> 4.15 us
    pallas_call x0 -> x1, Pallas kernels: none -> 37.5 us  [per_device(): pl.pallas_call(functools.partial(kernel, n_ep, n_tp, capacity), out_shape...]
    reduce_scatter x2 -> x0, waiting for transfers between devices: 34.2 us -> none  [the longest x1 20.8 us: per_device(): lax.psum_scatter(head_part.astype(jnp.bfloat16), 'tp', scatter_dimension=...]
    another operation x3 -> x0, other arithmetic: 20.1 us -> none
    dot_general x11 -> x0, matrix products: 16.2 us -> none  [the longest x1 3.42 us: stick_read(): jnp.einsum('tkgd,tlkd->tkgl', grouped, key_rows, preferred_element_type=j...]
    all_to_all x1 -> x0, blocking collectives: 12.8 us -> none  [per_device(): lax.all_to_all(outgoing, 'ep', split_axis=0, concat_axis=0, tiled=True)]
    all_gather x2 -> x0, blocking collectives: 11.9 us -> none  [the longest x1 6.49 us: per_device(): arrived = lax.all_gather(arrived, 'tp', axis=2, tiled=True)]
    all_to_all x1 -> x0, waiting for transfers between devices: 6.99 us -> none  [per_device(): lax.all_to_all(summed, 'ep', split_axis=0, concat_axis=0, tiled=True)]
    psum x1 -> x0, blocking collectives: 5.76 us -> none  [per_device(): squares = lax.psum(jnp.sum(mid_values * mid_values, axis=1), 'tp')]
  transfers between devices with their start and end apart: 3 -> 0, of which waited for: 3 -> 0; matrix products, arithmetic and copies ran while one was open for 2% -> 0% of each run, Pallas kernels for 0% -> 0%
where the time goes in v1:
time: 41.9 us; the launch traced here: 41.7 us
  Pallas kernels  37.5 us (89%)
  local copies, waits for them, and re-layouts  4.15 us (10%)
    pallas_call x1, Pallas kernels, per_device(): pl.pallas_call(functools.partial(kernel, n_ep, n_tp, capacity), out_shape...  37.5 us
    unnamed x1, local copies, waits for them, and re-layouts  1.38 us
    another operation x2, local copies, waits for them, and re-layouts, per_device(): jnp.tile(head_bias, seqs)[:, None]  1.36 us

profile of v1, /device:TPU:0, one launch (start us, length us, event | category | flops | bytes accessed | tf_op | source)
XLA Modules:
  0.0 41.7 jit_solution(13612839321499161281)
XLA Ops:
  0.0 0.7 %broadcast_in_dim.3 = s32[32,4]{1,0:T(8,128)S(1)} broadcast(s32[32]{0:T(128)} %param.17), dimensions={0} | broadcast | bytes 640 | tf_op jit(solution)/shard_map/broadcast_in_dim | solution.py:431
  0.7 0.7 %tile.2 = f32[32,4]{1,0:T(8,128)S(1)} broadcast(f32[4]{0:T(128)} %param.23), dimensions={1} | broadcast | bytes 528 | tf_op jit(solution)/shard_map/tile | solution.py:432
  1.4 0.7 %broadcast_in_dim_tile.4.bias_ref = f32[128,1]{1,0:T(8,128)} reshape(f32[32,4]{1,0:T(8,128)S(1)} %tile.2) | data formatting | bytes 1024 | tf_op jit(solution)/shard_map/broadcast_in_dim;tile | solution.py:432
  2.1 0.7 %broadcast_in_dim_reshape.4.lens_ref = s32[128,1]{1,0:T(8,128)} reshape(s32[32,4]{1,0:T(8,128)S(1)} %broadcast_in_dim.3) | data formatting | bytes 1024 | tf_op jit(solution)/shard_map/broadcast_in_dim;reshape | solution.py:431
  2.8 37.5 %decode_step.1 = bf16[32,512]{1,0:T(8,128)(2,1)} custom-call(s32[128,1]{1,0:T(8,128)} %broadcast_in_dim_reshape.4.lens_ref, f32[128,1]{1,0:T(8,128)} %broadcast_in_dim_tile.4.bias_ref, s32[4,32]{1,0:T(4,128)} %bitcast.19, bf16[8,2048]{1,0:T(8,128)(2,1)} %bitcast.15, bf16[1,2048]{1,0:T(2,128)(2,1)} %bitcast.16, f32[1,2048]{1,0:T(1,128)} %bitcast.17, ...), custom_call_target="tpu_custom_call" | custom-call | tf_op jit(solution)/shard_map/decode_step/pallas_call | solution.py:389
  40.3 1.4 %copy.21 = bf16[32,512]{1,0:T(8,128)(2,1)} copy(bf16[32,512]{1,0:T(8,128)(2,1)} %decode_step.1) | data formatting | bytes 65536

commit v2 on v1

--- a/solution.py
+++ b/solution.py
@@ -53,7 +53,7 @@
     diag = (near + 2) % n_tp
     seqs, width = res.shape
     own = width // n_tp
-    heads = bias_ref.shape[0] // seqs
+    heads = bias_ref.shape[1]
     size = keys.shape[2]
     experts = wexp_ref.shape[0]
 
@@ -82,7 +82,7 @@
         value_loads.append(
             pltpu.make_async_copy(value_hbm.at[rows], values.at[rows], value_sem.at[c])
         )
-    for copy in loads + weights[:1] + key_loads + value_loads + weights[1:]:
+    for copy in loads + weights[:1]:
         copy.start()
 
     barrier = pltpu.get_barrier_semaphore()
@@ -97,10 +97,14 @@
 
     for copy in loads:
         copy.wait()
+    for copy in key_loads:
+        copy.start()
     tokens = res[...].astype(F32)
     inverse = lax.rsqrt(jnp.sum(tokens * tokens, axis=1, keepdims=True) / width + EPSILON)
     normed = (tokens * inverse * mixg[...]).astype(BF)
     weights[0].wait()
+    for copy in value_loads + weights[1:2]:
+        copy.start()
     queries = jnp.dot(normed, wq[...], preferred_element_type=F32).astype(BF).astype(F32)
     for h in range(heads):
         qs[pl.ds(h, seqs, stride=heads), :] = queries[:, h * size:(h + 1) * size]
@@ -116,8 +120,26 @@
             total = term if total is None else jnp.where(row_of < j * heads, total, term)
         scores[t * heads:t * heads + 8, :] = total
     length = keys.shape[1]
-    z = scores[...] * size ** (-0.5) + bias_ref[...]
-    inside = lax.broadcasted_iota(jnp.int32, z.shape, 1) < lens_ref[...]
+    seq_of = lax.broadcasted_iota(jnp.int32, (seqs * heads, seqs), 0) // heads
+    lens = jnp.sum(
+        jnp.where(
+            seq_of == lax.broadcasted_iota(jnp.int32, seq_of.shape, 1),
+            lens_ref[...].astype(F32),
+            0.0,
+        ),
+        axis=1,
+        keepdims=True,
+    )
+    head_of = lax.broadcasted_iota(jnp.int32, (seqs * heads, heads), 0) % heads
+    bias = jnp.sum(
+        jnp.where(
+            head_of == lax.broadcasted_iota(jnp.int32, head_of.shape, 1), bias_ref[...], 0.0
+        ),
+        axis=1,
+        keepdims=True,
+    )
+    z = scores[...] * size ** (-0.5) + bias
+    inside = lax.broadcasted_iota(jnp.int32, z.shape, 1).astype(F32) < lens
     low = jnp.log1p(jnp.exp(-jnp.abs(z)))
     remain = jnp.where(inside, -(jnp.maximum(z, 0.0) + low), 0.0)
     after = (
@@ -142,19 +164,21 @@
         [att[pl.ds(h, seqs, stride=heads), :].astype(BF) for h in range(heads)], axis=1
     )
     weights[1].wait()
-    for p in range(n_tp):
-        head_send[p] = jnp.dot(
-            attended, wo[:, p * own:(p + 1) * own], preferred_element_type=F32
-        ).astype(BF)
+
+    def head_block(p):
+        columns = pl.ds(pl.multiple_of(p * own, own), own)
+        return jnp.dot(attended, wo[:, columns], preferred_element_type=F32).astype(BF)
 
     pl.semaphore_wait(barrier, n_tp - 1 + n_ep - 1)
     head_copies = []
-    for d in range(1, n_tp):
-        peer = lax.rem(tp + d, n_tp)
+    for d, peer in ((1, diag), (2, far), (3, near)):
+        head_send[peer] = head_block(peer)
         head_copies.append(
             remote(head_send.at[peer], head_recv.at[d], head_ss.at[d], head_rs.at[d], {"tp": peer})
         )
         head_copies[-1].start()
+    for copy in weights[2:]:
+        copy.start()
 
     routes = routes_ref[...]
     expert_row = lax.broadcasted_iota(jnp.int32, (experts, seqs), 0)
@@ -172,7 +196,7 @@
         jnp.broadcast_to(slot_of[:, None, :], slot_row.shape) == slot_row, 1.0, 0.0
     ).reshape(experts * capacity, seqs)
 
-    attn = head_send[tp].astype(F32)
+    attn = head_block(tp).astype(F32)
     for copy in head_copies:
         copy.wait_recv()
     for d in range(1, n_tp):
@@ -202,6 +226,7 @@
         mid_copies.append(
             remote(mid_all.at[tp], mid_all.at[tp], mid_ss.at[d], mid_rs.at[d], {"tp": peer})
         )
+        mid_copies[-1].start()
 
     def to_core(d):
         at = (tp, ep_source(d))
@@ -223,9 +248,6 @@
         dispatch(d).wait_recv()
         to_far(d).start()
         to_core(d).start()
-
-    for copy in mid_copies:
-        copy.start()
 
     @pl.loop(0, n_ep)
     def _(d):
@@ -428,8 +450,8 @@
         ),
         name="decode_step",
     )(
-        jnp.repeat(lengths, heads)[:, None],
-        jnp.tile(head_bias, seqs)[:, None],
+        lengths.reshape(1, seqs),
+        head_bias.reshape(1, heads),
         routes.T,
         w_expert.T,
         w_group.T,

time: 41.9 us -> 35.2 us (0.84)
  Pallas kernels: 37.5 us -> 33.6 us
  local copies, waits for them, and re-layouts: 4.15 us -> 1.38 us
    pallas_call x1, Pallas kernels: 37.5 us -> 33.6 us  [per_device(): pl.pallas_call(functools.partial(kernel, n_ep, n_tp, capacity), out_shape...]
    another operation x3 -> x0, local copies, waits for them, and re-layouts: 2.05 us -> none  [the longest x2 1.36 us: per_device(): jnp.tile(head_bias, seqs)[:, None]]
    broadcast_in_dim x1 -> x0, local copies, waits for them, and re-layouts: 0.72 us -> none  [per_device(): jnp.repeat(lengths, heads)[:, None]]
where the time goes in v2:
time: 35.2 us; the launch traced here: 35 us
  Pallas kernels  33.6 us (95%)
  local copies, waits for them, and re-layouts  1.38 us (4%)
    pallas_call x1, Pallas kernels, per_device(): pl.pallas_call(functools.partial(kernel, n_ep, n_tp, capacity), out_shape...  33.6 us
    unnamed x1, local copies, waits for them, and re-layouts  1.38 us

profile of v2, /device:TPU:0, one launch (start us, length us, event | category | flops | bytes accessed | tf_op | source)
XLA Modules:
  0.0 35.0 jit_solution(5032020304392889914)
XLA Ops:
  0.0 33.6 %decode_step.1 = bf16[32,512]{1,0:T(8,128)(2,1)} custom-call(s32[1,32]{1,0:T(1,128)} %bitcast.22, f32[1,4]{1,0:T(1,128)} %bitcast.23, s32[4,32]{1,0:T(4,128)} %bitcast.21, bf16[8,2048]{1,0:T(8,128)(2,1)} %bitcast.17, bf16[1,2048]{1,0:T(2,128)(2,1)} %bitcast.18, f32[1,2048]{1,0:T(1,128)} %bitcast.19, f32[1,2048]{1,0:T(1,128)} %bitcast.20, ...), custom_call_target="tpu_custom_call" | custom-call | tf_op jit(solution)/shard_map/decode_step/pallas_call | solution.py:411
  33.6 1.4 %copy.17 = bf16[32,512]{1,0:T(8,128)(2,1)} copy(bf16[32,512]{1,0:T(8,128)(2,1)} %decode_step.1) | data formatting | bytes 65536

commit v3 on v2

--- a/solution.py
+++ b/solution.py
@@ -58,19 +58,21 @@
     experts = wexp_ref.shape[0]
 
     def ep_peer(d):
-        return lax.rem(ep + d, n_ep)
-
-    def ep_source(d):
-        return lax.rem(ep + n_ep - d, n_ep)
+        peer, bit = 0, 1
+        while bit < n_ep:
+            peer = peer + (ep // bit + d // bit) % 2 * bit
+            bit *= 2
+        return peer
 
     loads = [
         pltpu.make_async_copy(src, dst, small_sem.at[i])
         for i, (src, dst) in enumerate(((res_hbm, res), (mixg_hbm, mixg), (moeg_hbm, moeg)))
     ]
+    top, end = pl.ds(0, width // 2), pl.ds(width // 2, width // 2)
     weights = [
         pltpu.make_async_copy(src, dst, weight_sem.at[i])
         for i, (src, dst) in enumerate(
-            ((wq_hbm, wq), (wo_hbm, wo), (wg_hbm, wg), (wu_hbm, wu), (wd_hbm, wd))
+            ((wq_hbm.at[top], wq.at[top]), (wq_hbm.at[end], wq.at[end]), (wo_hbm, wo), (wg_hbm, wg), (wu_hbm, wu), (wd_hbm, wd))
         )
     ]
     step = seqs // KEY_CHUNKS
@@ -82,7 +84,7 @@
         value_loads.append(
             pltpu.make_async_copy(value_hbm.at[rows], values.at[rows], value_sem.at[c])
         )
-    for copy in loads + weights[:1]:
+    for copy in loads + weights[:2]:
         copy.start()
 
     barrier = pltpu.get_barrier_semaphore()
@@ -103,9 +105,12 @@
     inverse = lax.rsqrt(jnp.sum(tokens * tokens, axis=1, keepdims=True) / width + EPSILON)
     normed = (tokens * inverse * mixg[...]).astype(BF)
     weights[0].wait()
-    for copy in value_loads + weights[1:2]:
+    queries = jnp.dot(normed[:, :width // 2], wq[top, :], preferred_element_type=F32)
+    weights[1].wait()
+    for copy in value_loads + weights[2:3]:
         copy.start()
-    queries = jnp.dot(normed, wq[...], preferred_element_type=F32).astype(BF).astype(F32)
+    queries = queries + jnp.dot(normed[:, width // 2:], wq[end, :], preferred_element_type=F32)
+    queries = queries.astype(BF).astype(F32)
     for h in range(heads):
         qs[pl.ds(h, seqs, stride=heads), :] = queries[:, h * size:(h + 1) * size]
     per = 8 // heads
@@ -163,7 +168,7 @@
     attended = jnp.concatenate(
         [att[pl.ds(h, seqs, stride=heads), :].astype(BF) for h in range(heads)], axis=1
     )
-    weights[1].wait()
+    weights[2].wait()
 
     def head_block(p):
         columns = pl.ds(pl.multiple_of(p * own, own), own)
@@ -177,7 +182,7 @@
             remote(head_send.at[peer], head_recv.at[d], head_ss.at[d], head_rs.at[d], {"tp": peer})
         )
         head_copies[-1].start()
-    for copy in weights[2:]:
+    for copy in weights[3:]:
         copy.start()
 
     routes = routes_ref[...]
@@ -217,7 +222,7 @@
 
     @pl.loop(1, n_ep)
     def _(d):
-        dispatch(d).start()
+        dispatch(n_ep - d).start()
 
     full[tp, ep] = slots[ep]
     mid_copies = []
@@ -229,15 +234,15 @@
         mid_copies[-1].start()
 
     def to_core(d):
-        at = (tp, ep_source(d))
+        at = (tp, ep_peer(d))
         return remote(full.at[at], full.at[at], core_ss.at[d], core_rs.at[d], {"tp": near})
 
     def to_far(d):
-        at = (tp, ep_source(d))
+        at = (tp, ep_peer(d))
         return remote(full.at[at], full.at[at], cross_ss.at[d], cross_rs.at[d], {"tp": far})
 
     def onward(d):
-        at = (far, ep_source(d))
+        at = (far, ep_peer(d))
         return remote(full.at[at], full.at[at], fwd_ss.at[d], fwd_rs.at[d], {"tp": near})
 
     to_far(0).start()
@@ -254,7 +259,7 @@
         to_far(d).wait_recv()
         onward(d).start()
 
-    for copy in weights[2:]:
+    for copy in weights[3:]:
         copy.wait()
 
     @pl.loop(0, n_ep)
@@ -299,14 +304,14 @@
     pair_send[...] = (far_part + part_recv[0].astype(F32)).astype(BF)
 
     def pair(d):
-        at = ep_source(d)
+        at = ep_peer(d)
         return remote(
             pair_send.at[at], pair_recv.at[at], pair_ss.at[d], pair_rs.at[d], {"tp": far}
         )
 
     @pl.loop(1, n_ep)
     def _(d):
-        pair(d).start()
+        pair(n_ep - d).start()
 
     pair(0).start()
     own_part = partial_of(tp).astype(F32)
@@ -314,7 +319,7 @@
     ret_send[...] = own_part + part_recv[1].astype(F32)
 
     def giving(d):
-        at = ep_source(d)
+        at = ep_peer(d)
         return remote(slots.at[at], ret_recv.at[ep], ret_ss.at[d], ret_rs.at[d], {"ep": at})
 
     @pl.loop(1, n_ep)
@@ -322,8 +327,9 @@
         dispatch(d).wait_send()
 
     @pl.loop(1, n_ep)
-    def _(d):
-        at = ep_source(d)
+    def _(i):
+        d = n_ep - i
+        at = ep_peer(d)
         pair(d).wait_recv()
         slots[at] = (ret_send[at] + pair_recv[at].astype(F32)).astype(BF)
         giving(d).start()
@@ -364,7 +370,7 @@
     @pl.loop(1, n_ep)
     def _(d):
         remote(
-            slots.at[ep], ret_recv.at[ep_peer(d)], ret_ss.at[d], ret_rs.at[d], {"ep": ep_source(d)}
+            slots.at[ep], ret_recv.at[ep_peer(d)], ret_ss.at[d], ret_rs.at[d], {"ep": ep_peer(d)}
         ).wait_recv()
 
     returned = ret_recv[...].reshape(experts * capacity, own)
@@ -439,7 +445,7 @@
             pltpu.VMEM((n_ep, capacity, own), BF),
             pltpu.VMEM((n_ep, capacity, own), F32),
             pltpu.VMEM((n_ep, capacity, own), BF),
-            dma((3,)), dma((5,)), dma((KEY_CHUNKS,)), dma((KEY_CHUNKS,)),
+            dma((3,)), dma((6,)), dma((KEY_CHUNKS,)), dma((KEY_CHUNKS,)),
             dma((n_tp,)), dma((n_tp,)), dma((n_tp,)), dma((n_tp,)),
             dma((n_ep,)), dma((n_ep,)),
             dma((n_ep,)), dma((n_ep,)), dma((n_ep,)), dma((n_ep,)), dma((n_ep,)), dma((n_ep,)),

time: 35.2 us -> 35.3 us (level)
  no operation moved by 1% of the time
where the time goes in v3:
time: 35.3 us; the launch traced here: 35 us
  Pallas kernels  33.6 us (95%)
  local copies, waits for them, and re-layouts  1.38 us (4%)
    pallas_call x1, Pallas kernels, per_device(): pl.pallas_call(functools.partial(kernel, n_ep, n_tp, capacity), out_shape...  33.6 us
    unnamed x1, local copies, waits for them, and re-layouts  1.38 us

profile of v3, /device:TPU:0, one launch (start us, length us, event | category | flops | bytes accessed | tf_op | source)
XLA Modules:
  0.0 35.0 jit_solution(1443972581636994972)
XLA Ops:
  0.0 33.6 %decode_step.1 = bf16[32,512]{1,0:T(8,128)(2,1)} custom-call(s32[1,32]{1,0:T(1,128)} %bitcast.22, f32[1,4]{1,0:T(1,128)} %bitcast.23, s32[4,32]{1,0:T(4,128)} %bitcast.21, bf16[8,2048]{1,0:T(8,128)(2,1)} %bitcast.17, bf16[1,2048]{1,0:T(2,128)(2,1)} %bitcast.18, f32[1,2048]{1,0:T(1,128)} %bitcast.19, f32[1,2048]{1,0:T(1,128)} %bitcast.20, ...), custom_call_target="tpu_custom_call" | custom-call | tf_op jit(solution)/shard_map/decode_step/pallas_call | solution.py:417
  33.6 1.4 %copy.17 = bf16[32,512]{1,0:T(8,128)(2,1)} copy(bf16[32,512]{1,0:T(8,128)(2,1)} %decode_step.1) | data formatting | bytes 65536
